TPU v7x, 32 devices: a whole 2x2x4 slice. The times are simulated.
32 devices in a mesh: ep: 8 (over z, y), tp: 4 (over x, core).
Axes of the slice: x: 2, y: 2, z: 4, core: 2. Of those that a mesh axis runs over, the one named last changes fastest.
Arguments:
- queries: bfloat16 [4096, 1024], P('ep', 'tp'), may hold values from -8 to 8
- key_rows: bfloat16 [4096, 1024], P('ep', 'tp'), may hold values from -8 to 8
- value_rows: bfloat16 [4096, 1024], P('ep', 'tp'), may hold values from -6 to 6
- lambdas: float32 [8], P('tp'), may hold values from 0.3 to 0.8
- head_gain: float32 [128], replicated, may hold values from 0.1 to 1.9
- out_weight: bfloat16 [1024, 2048], P('tp'), may hold values from -0.1875 to 0.1875
- moe_input: bfloat16 [4096, 2048], P(('ep', 'tp')), may hold values from -400 to 400
- moe_gain: float32 [2048], replicated, may hold values from 0.1 to 1.9
- routes: int32 [4096, 2], P(('ep', 'tp')), may hold values from 0 to 7, all different within a row; in each aligned block of 128 rows (0 to 127, 128 to 255, ...) at most 40 rows name the same one
- route_logits: float32 [4096, 2], P(('ep', 'tp')), may hold values from -6 to 6
- expert_gate: bfloat16 [8, 2048, 3584], P('ep', None, 'tp'), may hold values from -0.125 to 0.125
- expert_up: bfloat16 [8, 2048, 3584], P('ep', None, 'tp'), may hold values from -0.125 to 0.125
- expert_down: bfloat16 [8, 3584, 2048], P('ep', 'tp'), may hold values from -0.09375 to 0.09375
Outputs:
- mixer_out: bfloat16 [4096, 2048], P(('ep', 'tp'))
- expert_out: bfloat16 [4096, 2048], P(('ep', 'tp'))
Inputs may be any that keep to these rules, and one draw needn't show every extreme that they name: `routes`: each token names 2 different experts. Among the tokens of one device no expert is named more than 40 times, and in every draw some expert is named exactly 40 times by the tokens of some device.
All inputs are finite; a program needn't handle non-finite values.
Results may differ from a plain program's by a relative error of at most 0.014.
Values may be sent and summed in bfloat16 or wider, within the bound.
A program may use at most 128 MiB of HBM per device.

v0:
```python
import jax
import jax.numpy as jnp
from jax import lax
from jax.sharding import PartitionSpec as P

epsilon = 1e-06
init_lambda = 0.2


def capacity(tokens, top_count, experts):
    return max(2, (top_count * tokens * 5 + 4 * experts - 1) // (4 * experts))


def per_device(
    queries,
    key_rows,
    value_rows,
    lambdas,
    head_gain,
    out_weight,
    moe_input,
    moe_gain,
    routes,
    route_logits,
    expert_gate,
    expert_up,
    expert_down,
):
    local_rows = queries.shape[0]
    local_heads = lambdas.shape[0]
    head_size = queries.shape[1] // (2 * local_heads)
    value_size = value_rows.shape[1] // local_heads
    model_width = out_weight.shape[1]
    score_scale = head_size ** (-0.5)
    query_maps = queries.reshape(local_rows, local_heads, 2, head_size)

    def attend_block(running, key_block, value_block):
        maxima, totals, accumulated = running
        key_count = key_block.shape[0]
        key_maps = key_block.reshape(key_count, local_heads, 2, head_size)
        value_heads = value_block.reshape(key_count, local_heads, value_size)
        scores = (
            jnp.einsum("qhid,khid->ihqk", query_maps, key_maps, preferred_element_type=jnp.float32)
            * score_scale
        )
        new_max = jnp.maximum(maxima, jnp.max(scores, axis=-1))
        weights = jnp.exp(scores - new_max[..., None])
        factor = jnp.exp(maxima - new_max)
        totals = totals * factor + jnp.sum(weights, axis=-1)
        accumulated = accumulated * factor[..., None] + jnp.einsum(
            "ihqk,khe->ihqe",
            weights.astype(jnp.bfloat16),
            value_heads,
            preferred_element_type=jnp.float32,
        )
        return (new_max, totals, accumulated)

    initial = (
        jnp.full((2, local_heads, local_rows), -1e30, jnp.float32),
        jnp.zeros((2, local_heads, local_rows), jnp.float32),
        jnp.zeros((2, local_heads, local_rows, value_size), jnp.float32),
    )
    key_piece = lax.all_gather(key_rows, "ep", axis=0, tiled=True)
    value_piece = lax.all_gather(value_rows, "ep", axis=0, tiled=True)
    length = key_piece.shape[0]
    block_rows = length
    while block_rows > 1024 and block_rows % 2 == 0:
        block_rows //= 2

    def loop_body(step_index, partial_state):
        first_row = step_index * block_rows
        return attend_block(
            partial_state,
            lax.dynamic_slice_in_dim(key_piece, first_row, block_rows, 0),
            lax.dynamic_slice_in_dim(value_piece, first_row, block_rows, 0),
        )

    maxima, totals, accumulated = lax.fori_loop(0, length // block_rows, loop_body, initial)
    maps_out = accumulated / totals[..., None]
    head_out = maps_out[0] - lambdas[:, None, None] * maps_out[1]
    mean_square = jnp.mean(head_out * head_out, axis=-1, keepdims=True)
    attended = (
        head_out * lax.rsqrt(mean_square + epsilon) * head_gain * (1.0 - init_lambda)
    ).astype(jnp.bfloat16)
    out_heads = out_weight.reshape(local_heads, value_size, model_width)
    token_count, top_count = routes.shape
    experts_all = lax.axis_size("ep")
    slot_count = capacity(token_count, top_count, experts_all)
    moe_float = moe_input.astype(jnp.float32)
    normed = (
        moe_float
        * lax.rsqrt(jnp.mean(moe_float * moe_float, axis=-1, keepdims=True) + epsilon)
        * moe_gain
    ).astype(jnp.bfloat16)
    gate_weights = jax.nn.softmax(route_logits, axis=-1)
    flat_routes = routes.reshape(-1)
    chosen = (flat_routes[:, None] == jnp.arange(experts_all, dtype=jnp.int32)[None, :]).astype(
        jnp.int32
    )
    slot_rank = jnp.sum((jnp.cumsum(chosen, axis=0) - chosen) * chosen, axis=1)
    slot_ids = (flat_routes * slot_count + slot_rank).reshape(token_count, top_count)
    dispatch = jnp.any(
        slot_ids[None, :, :]
        == jnp.arange(experts_all * slot_count, dtype=jnp.int32)[:, None, None],
        axis=-1,
    ).astype(jnp.bfloat16)
    outgoing = (
        jnp.dot(dispatch, normed, preferred_element_type=jnp.float32)
        .astype(jnp.bfloat16)
        .reshape(experts_all, slot_count, model_width)
    )
    gate_local = expert_gate[0]
    up_local = expert_up[0]
    down_local = expert_down[0]
    arrived = lax.all_to_all(outgoing, "ep", split_axis=0, concat_axis=0, tiled=True)
    segment = lax.all_gather(
        arrived.reshape(experts_all * slot_count, model_width), "tp", axis=0, tiled=True
    )
    gate_part = jnp.dot(segment, gate_local, preferred_element_type=jnp.float32)
    up_part = jnp.dot(segment, up_local, preferred_element_type=jnp.float32)
    hidden = (jax.nn.silu(gate_part) * up_part).astype(jnp.bfloat16)
    expert_slots = experts_all * slot_count
    mixer_sum = lax.psum_scatter(
        jnp.einsum("hqe,hed->qd", attended, out_heads, preferred_element_type=jnp.float32).astype(
            jnp.bfloat16
        ),
        "tp",
        scatter_dimension=0,
        tiled=True,
    )
    expert_sum = lax.psum_scatter(
        jnp.dot(hidden, down_local, preferred_element_type=jnp.float32).astype(jnp.bfloat16),
        "tp",
        scatter_dimension=0,
        tiled=True,
    )
    replies = lax.all_to_all(
        expert_sum.reshape(experts_all, slot_count, model_width),
        "ep",
        split_axis=0,
        concat_axis=0,
        tiled=True,
    )
    picked = jnp.take(
        replies.reshape(expert_slots, model_width), slot_ids.reshape(-1), axis=0
    ).reshape(token_count, top_count, model_width)
    expert_out = jnp.sum(gate_weights[:, :, None] * picked.astype(jnp.float32), axis=1).astype(
        jnp.bfloat16
    )
    return (mixer_sum, expert_out)


def solution(mesh):
    placed = (
        P("ep", "tp"),
        P("ep", "tp"),
        P("ep", "tp"),
        P("tp"),
        P(),
        P("tp", None),
        P(("ep", "tp"), None),
        P(),
        P(("ep", "tp"), None),
        P(("ep", "tp"), None),
        P("ep", None, "tp"),
        P("ep", None, "tp"),
        P("ep", "tp", None),
    )
    return jax.shard_map(
        per_device,
        mesh=mesh,
        in_specs=placed,
        out_specs=(P(("ep", "tp"), None), P(("ep", "tp"), None)),
        check_vma=False,
    )
```

profile of v0, /device:TPU:0, one launch (start us, length us, event | category | flops | bytes accessed | tf_op | source)
XLA Modules:
  0.0 297.8 jit_solution(2833831292782214418)
XLA Ops:
  7.2 0.9 copy.64
  8.1 0.1 eq.39
  8.3 0.1 reshape.131
  8.4 0.6 reduce-window.6
  9.0 0.2 slice_reduce_fusion
  9.4 0.1 reduce_sum.65
  9.6 0.7 compare_and_fusion
  10.3 1.2 fusion.19
  11.6 1.6 convolution_convert_fusion.1
  13.2 38.6 %all_to_all.10 = bf16[8,40,2048]{2,1,0:T(8,128)(2,1)} all-to-all(bf16[8,40,2048]{2,1,0:T(8,128)(2,1)S(1)} %bitcast.102), channel_id=1, replica_groups=mesh['ep'=8,'tp'=4] {'ep'}, dimensions={0} | all-to-all | bytes 2621440 | tf_op jit(solution)/shard_map/all_to_all | solution.py:115
  51.9 0.8 copy.56
  52.8 0.8 copy.58
  53.7 37.7 %all-gather.8.cloned.1.call-done = bf16[1280,2048]{1,0:T(8,128)(2,1)} async-done(((bf16[320,2048]{1,0:T(8,128)(2,1)}), bf16[1280,2048]{1,0:T(8,128)(2,1)}) %all-gather.8.cloned.1.call-update) | async-done | bytes 5242896 | tf_op jit(solution)/shard_map/all_gather | solution.py:116
  91.4 10.0 %fusion.17 = f32[1280,896]{1,0:T(8,128)} fusion(bf16[1280,2048]{1,0:T(8,128)(2,1)} %all-gather.8.cloned.1.call-done, bf16[1,2048,896]{2,1,0:T(8,128)(2,1)} %param.25), kind=kOutput, calls=%fused_computation.25 | convolution fusion | flops 4697620480 | bytes 13500416 | tf_op jit(solution)/shard_map/dot_general | solution.py:119
  101.4 17.6 %convolution_convert_fusion = bf16[1280,2048]{1,0:T(8,128)(2,1)} fusion(bf16[1,896,2048]{2,1,0:T(8,128)(2,1)} %param.27, f32[1280,896]{1,0:T(8,128)} %fusion.17, bf16[1280,2048]{1,0:T(8,128)(2,1)} %all-gather.8.cloned.1.call-done, bf16[1,2048,896]{2,1,0:T(8,128)(2,1)} %param.26), kind=kOutput, calls=%fused_computation.20 | convolution fusion | flops 9404743680 | bytes 22413312 | tf_op jit(solution)/shard_map/dot_general | solution.py:132
  119.1 0.8 copy-done.3
  119.9 0.1 copy.57
  120.1 24.3 %all-gather.4.cloned.1.call-done = bf16[4096,256]{0,1:T(8,128)(2,1)} async-done(((bf16[512,256]{0,1:T(8,128)(2,1)}), bf16[4096,256]{0,1:T(8,128)(2,1)}) %all-gather.4.cloned.1.call-update) | async-done | bytes 2097168 | tf_op jit(solution)/shard_map/all_gather | solution.py:63
  144.4 51.2 %all-gather.6.cloned.1.call-done = bf16[4096,256]{0,1:T(8,128)(2,1)} async-done(((bf16[512,256]{0,1:T(8,128)(2,1)}), bf16[4096,256]{0,1:T(8,128)(2,1)}) %all-gather.6.cloned.1.call-update) | async-done | bytes 2097168 | tf_op jit(solution)/shard_map/all_gather | solution.py:64
  195.6 46.9 %while.18 = (s32[]{:T(128)}, f32[2,2,512]{2,1,0:T(2,128)S(1)}, f32[2,2,512]{2,1,0:T(2,128)S(1)}, f32[2,2,512,128]{2,3,0,1:T(8,128)S(1)}, bf16[4096,256]{0,1:T(8,...) while((s32[]{:T(128)}, f32[2,2,512]{2,1,0:T(2,128)S(1)}, ...), condition=%wide.region_3.0_spmd.clone, body=%wide.region_0.0_spmd.clone.sunk | while | flops 818685952 | bytes 30810288 | solution.py:78
  195.6 1.3 constant_dynamic-slice_fusion.3
  196.9 4.6 %bitcast_reduce_fusion.2 = (f32[2,2,512]{2,1,0:T(2,128)S(1)}, f32[2,2,1024,512]{3,2,1,0:T(8,128)}) fusion(bf16[512,2,2,64]{0,3,1,2:T(8,128)(2,1)S(1)} %get-tuple-element.284, bf16[1024,2,2,64]{0,3,2,1:T(8,128)(2,1)S(1)} %bitcast.99), kind=kOutput, calls=%fused_computation.2.clone.1 | convolution fusion | flops 272627712 | bytes 9183232 | tf_op jit(solution)/shard_map/while/body/eval_jaxpr/qhid,khid->ihqk/dot_general | solution.py:43
  201.5 5.4 %fusion.66 = (bf16[2,2,512,1024]{2,3,1,0:T(8,128)(2,1)S(1)}, f32[2,2,512]{2,1,0:T(2,128)S(1)}) fusion(f32[2,2,1024,512]{3,2,1,0:T(8,128)} %get-tuple-element.251, f32[2,2,512]{2,1,0:T(2,128)S(1)} %fusion.65), kind=kLoop, calls=%fused_computation.4.clone.1 | loop fusion | flops 8386560 | bytes 12599296 | tf_op jit(solution)/shard_map/while/body/eval_jaxpr/convert_element_type | solution.py:52
  207.0 0.9 fusion.68
  207.9 1.3 constant_dynamic-slice_fusion.3
  209.2 4.6 %bitcast_reduce_fusion.2 = (f32[2,2,512]{2,1,0:T(2,128)S(1)}, f32[2,2,1024,512]{3,2,1,0:T(8,128)}) fusion(bf16[512,2,2,64]{0,3,1,2:T(8,128)(2,1)S(1)} %get-tuple-element.284, bf16[1024,2,2,64]{0,3,2,1:T(8,128)(2,1)S(1)} %bitcast.99), kind=kOutput, calls=%fused_computation.2.clone.1 | convolution fusion | flops 272627712 | bytes 9183232 | tf_op jit(solution)/shard_map/while/body/eval_jaxpr/qhid,khid->ihqk/dot_general | solution.py:43
  213.9 5.1 %fusion.66 = (bf16[2,2,512,1024]{2,3,1,0:T(8,128)(2,1)S(1)}, f32[2,2,512]{2,1,0:T(2,128)S(1)}) fusion(f32[2,2,1024,512]{3,2,1,0:T(8,128)} %get-tuple-element.251, f32[2,2,512]{2,1,0:T(2,128)S(1)} %fusion.65), kind=kLoop, calls=%fused_computation.4.clone.1 | loop fusion | flops 8386560 | bytes 12599296 | tf_op jit(solution)/shard_map/while/body/eval_jaxpr/convert_element_type | solution.py:52
  219.1 0.9 fusion.68
  220.0 1.3 constant_dynamic-slice_fusion.3
  221.3 4.6 %bitcast_reduce_fusion.2 = (f32[2,2,512]{2,1,0:T(2,128)S(1)}, f32[2,2,1024,512]{3,2,1,0:T(8,128)}) fusion(bf16[512,2,2,64]{0,3,1,2:T(8,128)(2,1)S(1)} %get-tuple-element.284, bf16[1024,2,2,64]{0,3,2,1:T(8,128)(2,1)S(1)} %bitcast.99), kind=kOutput, calls=%fused_computation.2.clone.1 | convolution fusion | flops 272627712 | bytes 9183232 | tf_op jit(solution)/shard_map/while/body/eval_jaxpr/qhid,khid->ihqk/dot_general | solution.py:43
  225.9 4.3 %fusion.66 = (bf16[2,2,512,1024]{2,3,1,0:T(8,128)(2,1)S(1)}, f32[2,2,512]{2,1,0:T(2,128)S(1)}) fusion(f32[2,2,1024,512]{3,2,1,0:T(8,128)} %get-tuple-element.251, f32[2,2,512]{2,1,0:T(2,128)S(1)} %fusion.65), kind=kLoop, calls=%fused_computation.4.clone.1 | loop fusion | flops 8386560 | bytes 12599296 | tf_op jit(solution)/shard_map/while/body/eval_jaxpr/convert_element_type | solution.py:52
  230.3 0.9 fusion.68
  231.3 1.3 constant_dynamic-slice_fusion.3
  232.6 4.6 %bitcast_reduce_fusion.2 = (f32[2,2,512]{2,1,0:T(2,128)S(1)}, f32[2,2,1024,512]{3,2,1,0:T(8,128)}) fusion(bf16[512,2,2,64]{0,3,1,2:T(8,128)(2,1)S(1)} %get-tuple-element.284, bf16[1024,2,2,64]{0,3,2,1:T(8,128)(2,1)S(1)} %bitcast.99), kind=kOutput, calls=%fused_computation.2.clone.1 | convolution fusion | flops 272627712 | bytes 9183232 | tf_op jit(solution)/shard_map/while/body/eval_jaxpr/qhid,khid->ihqk/dot_general | solution.py:43
  237.2 4.3 %fusion.66 = (bf16[2,2,512,1024]{2,3,1,0:T(8,128)(2,1)S(1)}, f32[2,2,512]{2,1,0:T(2,128)S(1)}) fusion(f32[2,2,1024,512]{3,2,1,0:T(8,128)} %get-tuple-element.251, f32[2,2,512]{2,1,0:T(2,128)S(1)} %fusion.65), kind=kLoop, calls=%fused_computation.4.clone.1 | loop fusion | flops 8386560 | bytes 12599296 | tf_op jit(solution)/shard_map/while/body/eval_jaxpr/convert_element_type | solution.py:52
  241.5 0.9 fusion.68
  242.5 0.1 broadcast_divide_fusion
  242.6 0.2 multiply_reduce_fusion.1
  242.9 2.2 bitcast_convert_fusion
  245.1 2.4 reduce-scatter.5.cloned.1.call-done
  247.5 5.5 %all-to-all-start.1 = ((bf16[8,40,2048]{2,1,0:T(8,128)(2,1)}), bf16[8,40,2048]{2,1,0:T(8,128)(2,1)S(1)}, u32[]{:S(2)}, u32[]{:S(2)}) async-start(bf16[8,40,2048]{2,1,0:T(8,128)(2,1)} %bitcast.103), calls=%async_computation.3 | async-start | bytes 2621440 | tf_op jit(solution)/shard_map/all_to_all | solution.py:137
  253.2 0.1 mul.155
  253.3 0.1 copy.67
  253.5 0.1 copy.63
  253.7 30.6 %all-to-all-done.1 = bf16[8,40,2048]{2,1,0:T(8,128)(2,1)S(1)} async-done(((bf16[8,40,2048]{2,1,0:T(8,128)(2,1)}), bf16[8,40,2048]{2,1,0:T(8,128)(2,1)S(1)}, u32[]{:S(2)}, u32[]{:S(2)}) %all-to-all-start.1) | async-done | bytes 1310752 | tf_op jit(solution)/shard_map/all_to_all | solution.py:137
  284.3 1.4 gather_fusion
  285.6 0.7 gather.7
  286.4 4.9 %multiply_reduce_fusion = bf16[128,2048]{1,0:T(8,128)(2,1)} fusion(bf16[128,2,2048]{2,1,0:T(2,128)(2,1)S(1)} %gather.7, pred[128,2]{1,0:T(8,128)(4,1)S(1)} %copy.67, f32[128,2]{1,0:T(8,128)S(1)} %copy.63), kind=kLoop, calls=%fused_computation.28 | loop fusion | flops 1835008 | bytes 1574144 | tf_op jit(solution)/shard_map/reduce_sum | solution.py:147
  (62 shorter events, 1.0 us)
Async XLA Ops:
  7.2 235.7 %copy-start = (bf16[256,2048]{1,0:T(8,128)(2,1)S(1)}, bf16[256,2048]{1,0:T(8,128)(2,1)}, u32[]{:S(2)}) copy-start(bf16[256,2048]{1,0:T(8,128)(2,1)} %param.20) | copy-start | bytes 3145732
  7.2 44.7 %copy-start.1 = (bf16[512,256]{1,0:T(8,128)(2,1)S(1)}, bf16[512,256]{1,0:T(8,128)(2,1)}, u32[]{:S(2)}) copy-start(bf16[512,256]{1,0:T(8,128)(2,1)} %param.16) | copy-start | bytes 786436
  7.2 45.6 %copy-start.2 = (bf16[512,256]{1,0:T(8,128)(2,1)S(1)}, bf16[512,256]{1,0:T(8,128)(2,1)}, u32[]{:S(2)}) copy-start(bf16[512,256]{1,0:T(8,128)(2,1)} %param.17) | copy-start | bytes 786436
  7.2 84.2 %all-gather.8.cloned.1.call-start = ((), (), s32[]{:S(2)}) async-start(), calls=%async_computation.7 | async-start | bytes 6553600 | tf_op jit(solution)/shard_map/all_gather | solution.py:116
  51.8 92.6 %all-gather.4.cloned.1.call-start = ((), (), s32[]{:S(2)}) async-start(), calls=%async_computation.4 | async-start | bytes 2359296 | tf_op jit(solution)/shard_map/all_gather | solution.py:63
  52.8 142.8 %all-gather.6.cloned.1.call-start = ((), (), s32[]{:S(2)}) async-start(), calls=%async_computation.5 | async-start | bytes 2359296 | tf_op jit(solution)/shard_map/all_gather | solution.py:64
  53.7 193.9 %reduce-scatter.5.cloned.1.call-start = ((), (), s32[]{:S(2)}) async-start(), calls=%async_computation.8 | async-start | bytes 6553600 | tf_op jit(solution)/shard_map/reduce_scatter | solution.py:131
  119.0 0.9 copy-start.3
  119.0 172.3 %reduce-scatter.3.cloned.1.call-start = ((), (), s32[]{:S(2)}) async-start(), calls=%async_computation.6 | async-start | bytes 2621440 | tf_op jit(solution)/shard_map/reduce_scatter | solution.py:123
  195.6 47.0 %copy-start.6 = (f32[2]{0:T(128)S(1)}, f32[2]{0:T(128)}, u32[]{:S(2)}) copy-start(f32[2]{0:T(128)} %param.18) | copy-start | bytes 28
  195.6 47.3 %copy-start.7 = (f32[128]{0:T(128)S(1)}, f32[128]{0:T(128)}, u32[]{:S(2)}) copy-start(f32[128]{0:T(128)} %param.19) | copy-start | bytes 1540
  242.8 10.2 %copy-start.4 = (s32[128,2]{0,1:T(2,128)S(1)}, s32[128,2]{0,1:T(2,128)}, u32[]{:S(2)}) copy-start(s32[128,2]{0,1:T(2,128)} %param.23) | copy-start | bytes 3076
  242.8 10.6 %copy-start.5 = (f32[128,2]{0,1:T(2,128)S(1)}, f32[128,2]{0,1:T(2,128)}, u32[]{:S(2)}) copy-start(f32[128,2]{0,1:T(2,128)} %param.24) | copy-start | bytes 3076
  247.5 36.7 %all-to-all-start.1 = ((bf16[8,40,2048]{2,1,0:T(8,128)(2,1)}), bf16[8,40,2048]{2,1,0:T(8,128)(2,1)S(1)}, u32[]{:S(2)}, u32[]{:S(2)}) async-start(bf16[8,40,2048]{2,1,0:T(8,128)(2,1)} %bitcast.103), calls=%async_computation.3 | async-start | bytes 2621440 | tf_op jit(solution)/shard_map/all_to_all | solution.py:137
Sparse Core Ops, SparseCore 0:
  51.9 39.4 all-gather.7
  94.0 50.3 all-gather.3
  147.0 48.5 all-gather.5
  198.0 49.5 reduce-scatter.4
  250.5 31.1 reduce-scatter.2
where the time goes:
time: 298 us
  waiting for transfers between devices  146 us (49%)
  matrix products  53.6 us (18%)
  blocking collectives  38.6 us (13%)
  other arithmetic  27.3 us (9%)
  between operations  14 us (5%)
  local copies, waits for them, and re-layouts  12.1 us (4%)
  starting transfers between devices  5.71 us (2%)
    all_gather x1, waiting for transfers between devices, per_device(): value_piece = lax.all_gather(value_rows, 'ep', axis=0, tiled=True)  51.2 us
    all_to_all x1, blocking collectives, per_device(): lax.all_to_all(outgoing, 'ep', split_axis=0, concat_axis=0, tiled=True)  38.6 us
    all_gather x1, waiting for transfers between devices, per_device(): lax.all_gather(arrived.reshape(experts_all * slot_count, model_width), 't...  37.7 us
    all_to_all x1, waiting for transfers between devices, per_device(): lax.all_to_all(expert_sum.reshape(experts_all, slot_count, model_width),...  30.6 us
    all_gather x1, waiting for transfers between devices, per_device(): key_piece = lax.all_gather(key_rows, 'ep', axis=0, tiled=True)  24.3 us
    convert_element_type x4, other arithmetic, attend_block(): weights.astype(jnp.bfloat16)  19.1 us
    dot_general x4, matrix products, attend_block(): jnp.einsum('qhid,khid->ihqk', query_maps, key_maps, preferred_element_typ...  18.5 us
    dot_general x1, matrix products, per_device(): jnp.dot(hidden, down_local, preferred_element_type=jnp.float32)  17.6 us
  transfers between devices with their start and end apart: 6, of which 5 were waited for; matrix products, arithmetic and copies ran while one was open for 29% of the time, Pallas kernels for 0%

commit v1 on v0

--- a/solution.py
+++ b/solution.py
@@ -61,7 +61,13 @@
         jnp.zeros((2, local_heads, local_rows, value_size), jnp.float32),
     )
     key_piece = lax.all_gather(key_rows, "ep", axis=0, tiled=True)
-    value_piece = lax.all_gather(value_rows, "ep", axis=0, tiled=True)
+    peers = lax.axis_size("ep")
+    current, parts = (value_rows, [value_rows])
+    for _ in range(peers - 1):
+        current = lax.ppermute(current, "ep", [(i, (i + 1) % peers) for i in range(peers)])
+        parts.insert(0, current)
+    row_of_blocks = jnp.concatenate(parts, axis=0)
+    value_piece = jnp.roll(row_of_blocks, (lax.axis_index("ep") + 1) * value_rows.shape[0], axis=0)
     length = key_piece.shape[0]
     block_rows = length
     while block_rows > 1024 and block_rows % 2 == 0:

time: 298 us -> 267 us (0.90)
  waiting for transfers between devices: 146 us -> 93.2 us
  local copies, waits for them, and re-layouts: 12.1 us -> 35.9 us
    ppermute x0 -> x7, waiting for transfers between devices: none -> 63.4 us  [per_device(): lax.ppermute(current, 'ep', [(i, (i + 1) % peers) for i in range(peers)])]
    all_gather x1 -> x0, waiting for transfers between devices: 51.2 us -> none  [per_device(): value_piece = lax.all_gather(value_rows, 'ep', axis=0, tiled=True)]
    all_gather x1, waiting for transfers between devices: 37.7 us -> 0.01 us  [per_device(): lax.all_gather(arrived.reshape(experts_all * slot_count, model_width), 't...]
    all_gather x1, waiting for transfers between devices: 24.3 us -> 0.01 us  [per_device(): key_piece = lax.all_gather(key_rows, 'ep', axis=0, tiled=True)]
    unnamed x21 -> x38, local copies, waits for them, and re-layouts: 3.62 us -> 23.5 us
    dynamic_slice x0 -> x1, local copies, waits for them, and re-layouts: none -> 3.16 us  [per_device(): jnp.roll(row_of_blocks, (lax.axis_index('ep') + 1) * value_rows.shape[0],...]
  transfers between devices with their start and end apart: 6 -> 12, of which waited for: 5 -> 8; matrix products, arithmetic and copies ran while one was open for 29% -> 41% of each run, Pallas kernels for 0% -> 0%
where the time goes in v1:
time: 267 us
  waiting for transfers between devices  93.2 us (35%)
  matrix products  54 us (20%)
  blocking collectives  38.6 us (14%)
  local copies, waits for them, and re-layouts  35.9 us (13%)
  other arithmetic  25.3 us (9%)
  between operations  14.1 us (5%)
  starting transfers between devices  5.41 us (2%)
    ppermute x7, waiting for transfers between devices, per_device(): lax.ppermute(current, 'ep', [(i, (i + 1) % peers) for i in range(peers)])  63.4 us
    all_to_all x1, blocking collectives, per_device(): lax.all_to_all(outgoing, 'ep', split_axis=0, concat_axis=0, tiled=True)  38.6 us
    all_to_all x1, waiting for transfers between devices, per_device(): lax.all_to_all(expert_sum.reshape(experts_all, slot_count, model_width),...  29.7 us
    unnamed x38, local copies, waits for them, and re-layouts  23.5 us
    dot_general x4, matrix products, attend_block(): jnp.einsum('qhid,khid->ihqk', query_maps, key_maps, preferred_element_typ...  18.6 us
    dot_general x1, matrix products, per_device(): jnp.dot(hidden, down_local, preferred_element_type=jnp.float32)  17.8 us
    convert_element_type x4, other arithmetic, attend_block(): weights.astype(jnp.bfloat16)  17.2 us
    dot_general x1, matrix products, per_device(): gate_part = jnp.dot(segment, gate_local, preferred_element_type=jnp.float32)  10 us
  transfers between devices with their start and end apart: 12, of which 8 were waited for; matrix products, arithmetic and copies ran while one was open for 41% of the time, Pallas kernels for 0%

profile of v1, /device:TPU:0, one launch (start us, length us, event | category | flops | bytes accessed | tf_op | source)
XLA Modules:
  0.0 266.7 jit_solution(305701796914433798)
XLA Ops:
  7.2 0.9 copy.72
  10.3 1.2 fusion.19
  11.6 1.6 convolution_convert_fusion.1
  13.2 38.6 %all_to_all.10 = bf16[8,40,2048]{2,1,0:T(8,128)(2,1)} all-to-all(bf16[8,40,2048]{2,1,0:T(8,128)(2,1)S(1)} %bitcast.102), channel_id=1, replica_groups=mesh['ep'=8,'tp'=4] {'ep'}, dimensions={0} | all-to-all | bytes 2621440 | tf_op jit(solution)/shard_map/all_to_all | solution.py:121
  52.0 1.5 collective-permute-start
  53.5 8.1 %collective-permute-done = bf16[512,256]{0,1:T(8,128)(2,1)S(1)} collective-permute-done((bf16[512,256]{0,1:T(8,128)(2,1)S(1)}, bf16[512,256]{0,1:T(8,128)(2,1)S(1)}, u32[]{:S(2)}, u32[]{:S(2)}) %collective-permute-start) | collective-permute-done | bytes 262176 | tf_op jit(solution)/shard_map/ppermute | solution.py:67
  61.6 9.1 %collective-permute-done.1 = bf16[512,256]{0,1:T(8,128)(2,1)S(1)} collective-permute-done((bf16[512,256]{0,1:T(8,128)(2,1)S(1)}, bf16[512,256]{0,1:T(8,128)(2,1)S(1)}, u32[]{:S(2)}, u32[]{:S(2)}) %collective-permute-start.1) | collective-permute-done | bytes 262176 | tf_op jit(solution)/shard_map/ppermute | solution.py:67
  70.7 9.1 %collective-permute-done.2 = bf16[512,256]{0,1:T(8,128)(2,1)S(1)} collective-permute-done((bf16[512,256]{0,1:T(8,128)(2,1)S(1)}, bf16[512,256]{0,1:T(8,128)(2,1)S(1)}, u32[]{:S(2)}, u32[]{:S(2)}) %collective-permute-start.2) | collective-permute-done | bytes 262176 | tf_op jit(solution)/shard_map/ppermute | solution.py:67
  79.8 9.4 %collective-permute-done.3 = bf16[512,256]{0,1:T(8,128)(2,1)S(1)} collective-permute-done((bf16[512,256]{0,1:T(8,128)(2,1)S(1)}, bf16[512,256]{0,1:T(8,128)(2,1)S(1)}, u32[]{:S(2)}, u32[]{:S(2)}) %collective-permute-start.3) | collective-permute-done | bytes 262176 | tf_op jit(solution)/shard_map/ppermute | solution.py:67
  89.2 10.6 %collective-permute-done.4 = bf16[512,256]{0,1:T(8,128)(2,1)S(1)} collective-permute-done((bf16[512,256]{0,1:T(8,128)(2,1)S(1)}, bf16[512,256]{0,1:T(8,128)(2,1)S(1)}, u32[]{:S(2)}, u32[]{:S(2)}) %collective-permute-start.4) | collective-permute-done | bytes 262176 | tf_op jit(solution)/shard_map/ppermute | solution.py:67
  99.8 11.5 %collective-permute-done.5 = bf16[512,256]{0,1:T(8,128)(2,1)} collective-permute-done((bf16[512,256]{0,1:T(8,128)(2,1)S(1)}, bf16[512,256]{0,1:T(8,128)(2,1)}, u32[]{:S(2)}, u32[]{:S(2)}) %collective-permute-start.5) | collective-permute-done | bytes 262176 | tf_op jit(solution)/shard_map/ppermute | solution.py:67
  111.3 0.8 copy.62
  112.3 1.8 copy.63
  114.1 1.0 copy.67
  115.1 5.6 %collective-permute-done.6 = bf16[512,256]{0,1:T(8,128)(2,1)} collective-permute-done((bf16[512,256]{0,1:T(8,128)(2,1)}, bf16[512,256]{0,1:T(8,128)(2,1)}, u32[]{:S(2)}, u32[]{:S(2)}) %collective-permute-start.6) | collective-permute-done | bytes 262176 | tf_op jit(solution)/shard_map/ppermute | solution.py:67
  120.7 1.7 constant_dynamic-update-slice_fusion.15
  122.4 1.7 constant_dynamic-update-slice_fusion.14
  124.1 1.7 constant_dynamic-update-slice_fusion.13
  125.9 1.7 constant_dynamic-update-slice_fusion.12
  130.6 10.0 %fusion.17 = f32[1280,896]{1,0:T(8,128)} fusion(bf16[1280,2048]{1,0:T(8,128)(2,1)} %all-gather.5.cloned.1.call-done, bf16[1,2048,896]{2,1,0:T(8,128)(2,1)} %param.25), kind=kOutput, calls=%fused_computation.25 | convolution fusion | flops 4697620480 | bytes 13500416 | tf_op jit(solution)/shard_map/dot_general | solution.py:125
  140.6 17.8 %convolution_convert_fusion = bf16[1280,2048]{1,0:T(8,128)(2,1)} fusion(bf16[1,896,2048]{2,1,0:T(8,128)(2,1)} %param.27, f32[1280,896]{1,0:T(8,128)} %fusion.17, bf16[1280,2048]{1,0:T(8,128)(2,1)} %all-gather.5.cloned.1.call-done, bf16[1,2048,896]{2,1,0:T(8,128)(2,1)} %param.26), kind=kOutput, calls=%fused_computation.20 | convolution fusion | flops 9404743680 | bytes 22413312 | tf_op jit(solution)/shard_map/dot_general | solution.py:138
  158.6 1.7 constant_dynamic-update-slice_fusion.7
  160.3 1.7 constant_dynamic-update-slice_fusion.6
  162.0 1.7 constant_dynamic-update-slice_fusion.5
  163.7 1.7 constant_dynamic-update-slice_fusion.4
  168.4 3.2 %constant_dynamic-slice_fusion.2 = bf16[4096,256]{0,1:T(8,128)(2,1)} fusion(bf16[8192,256]{0,1:T(8,128)(2,1)} %constant_dynamic-update-slice_fusion, s32[]{:T(128)S(6)} %select_n.44), kind=kLoop, calls=%fused_computation.82 | loop fusion | bytes 4194308 | tf_op jit(solution)/shard_map/jit(_roll_dynamic)/dynamic_slice | solution.py:70
  171.5 45.0 %while.18 = (s32[]{:T(128)}, f32[2,2,512]{2,1,0:T(2,128)S(1)}, f32[2,2,512]{2,1,0:T(2,128)S(1)}, f32[2,2,512,128]{2,3,0,1:T(8,128)S(1)}, bf16[4096,256]{0,1:T(8,...) while((s32[]{:T(128)}, f32[2,2,512]{2,1,0:T(2,128)S(1)}, ...), condition=%wide.region_3.4_spmd.clone, body=%wide.region_0.3_spmd.clone.sunk | while | flops 818685952 | bytes 30810280 | solution.py:84
  171.5 1.3 constant_dynamic-slice_fusion.4
  172.8 4.8 %bitcast_reduce_fusion.2 = (f32[2,2,512]{2,1,0:T(2,128)S(1)}, f32[2,2,1024,512]{3,2,1,0:T(8,128)}) fusion(bf16[512,2,2,64]{0,3,1,2:T(8,128)(2,1)S(1)} %get-tuple-element.284, bf16[1024,2,2,64]{0,3,2,1:T(8,128)(2,1)S(1)} %bitcast.99), kind=kOutput, calls=%fused_computation.2.clone.1 | convolution fusion | flops 272627712 | bytes 9183232 | tf_op jit(solution)/shard_map/while/body/eval_jaxpr/qhid,khid->ihqk/dot_general | solution.py:43
  177.6 4.3 %fusion.66 = (bf16[2,2,512,1024]{2,3,1,0:T(8,128)(2,1)S(1)}, f32[2,2,512]{2,1,0:T(2,128)S(1)}) fusion(f32[2,2,1024,512]{3,2,1,0:T(8,128)} %get-tuple-element.251, f32[2,2,512]{2,1,0:T(2,128)S(1)} %fusion.65), kind=kLoop, calls=%fused_computation.4.clone.1 | loop fusion | flops 8386560 | bytes 12599296 | tf_op jit(solution)/shard_map/while/body/eval_jaxpr/convert_element_type | solution.py:52
  182.0 0.9 fusion.68
  182.9 1.3 constant_dynamic-slice_fusion.4
  184.2 4.6 %bitcast_reduce_fusion.2 = (f32[2,2,512]{2,1,0:T(2,128)S(1)}, f32[2,2,1024,512]{3,2,1,0:T(8,128)}) fusion(bf16[512,2,2,64]{0,3,1,2:T(8,128)(2,1)S(1)} %get-tuple-element.284, bf16[1024,2,2,64]{0,3,2,1:T(8,128)(2,1)S(1)} %bitcast.99), kind=kOutput, calls=%fused_computation.2.clone.1 | convolution fusion | flops 272627712 | bytes 9183232 | tf_op jit(solution)/shard_map/while/body/eval_jaxpr/qhid,khid->ihqk/dot_general | solution.py:43
  188.8 4.3 %fusion.66 = (bf16[2,2,512,1024]{2,3,1,0:T(8,128)(2,1)S(1)}, f32[2,2,512]{2,1,0:T(2,128)S(1)}) fusion(f32[2,2,1024,512]{3,2,1,0:T(8,128)} %get-tuple-element.251, f32[2,2,512]{2,1,0:T(2,128)S(1)} %fusion.65), kind=kLoop, calls=%fused_computation.4.clone.1 | loop fusion | flops 8386560 | bytes 12599296 | tf_op jit(solution)/shard_map/while/body/eval_jaxpr/convert_element_type | solution.py:52
  193.1 0.9 fusion.68
  194.1 1.3 constant_dynamic-slice_fusion.4
  195.4 4.6 %bitcast_reduce_fusion.2 = (f32[2,2,512]{2,1,0:T(2,128)S(1)}, f32[2,2,1024,512]{3,2,1,0:T(8,128)}) fusion(bf16[512,2,2,64]{0,3,1,2:T(8,128)(2,1)S(1)} %get-tuple-element.284, bf16[1024,2,2,64]{0,3,2,1:T(8,128)(2,1)S(1)} %bitcast.99), kind=kOutput, calls=%fused_computation.2.clone.1 | convolution fusion | flops 272627712 | bytes 9183232 | tf_op jit(solution)/shard_map/while/body/eval_jaxpr/qhid,khid->ihqk/dot_general | solution.py:43
  200.0 4.4 %fusion.66 = (bf16[2,2,512,1024]{2,3,1,0:T(8,128)(2,1)S(1)}, f32[2,2,512]{2,1,0:T(2,128)S(1)}) fusion(f32[2,2,1024,512]{3,2,1,0:T(8,128)} %get-tuple-element.251, f32[2,2,512]{2,1,0:T(2,128)S(1)} %fusion.65), kind=kLoop, calls=%fused_computation.4.clone.1 | loop fusion | flops 8386560 | bytes 12599296 | tf_op jit(solution)/shard_map/while/body/eval_jaxpr/convert_element_type | solution.py:52
  204.4 0.9 fusion.68
  205.4 1.3 constant_dynamic-slice_fusion.4
  206.6 4.6 %bitcast_reduce_fusion.2 = (f32[2,2,512]{2,1,0:T(2,128)S(1)}, f32[2,2,1024,512]{3,2,1,0:T(8,128)}) fusion(bf16[512,2,2,64]{0,3,1,2:T(8,128)(2,1)S(1)} %get-tuple-element.284, bf16[1024,2,2,64]{0,3,2,1:T(8,128)(2,1)S(1)} %bitcast.99), kind=kOutput, calls=%fused_computation.2.clone.1 | convolution fusion | flops 272627712 | bytes 9183232 | tf_op jit(solution)/shard_map/while/body/eval_jaxpr/qhid,khid->ihqk/dot_general | solution.py:43
  211.2 4.3 %fusion.66 = (bf16[2,2,512,1024]{2,3,1,0:T(8,128)(2,1)S(1)}, f32[2,2,512]{2,1,0:T(2,128)S(1)}) fusion(f32[2,2,1024,512]{3,2,1,0:T(8,128)} %get-tuple-element.251, f32[2,2,512]{2,1,0:T(2,128)S(1)} %fusion.65), kind=kLoop, calls=%fused_computation.4.clone.1 | loop fusion | flops 8386560 | bytes 12599296 | tf_op jit(solution)/shard_map/while/body/eval_jaxpr/convert_element_type | solution.py:52
  215.6 0.9 fusion.68
  216.9 2.2 bitcast_convert_fusion
  219.2 3.6 %all-to-all-start.1 = ((bf16[8,40,2048]{2,1,0:T(8,128)(2,1)}), bf16[8,40,2048]{2,1,0:T(8,128)(2,1)S(1)}, u32[]{:S(2)}, u32[]{:S(2)}) async-start(bf16[8,40,2048]{2,1,0:T(8,128)(2,1)} %bitcast.103), calls=%async_computation.3 | async-start | bytes 2621440 | tf_op jit(solution)/shard_map/all_to_all | solution.py:143
  223.4 29.7 %all-to-all-done.1 = bf16[8,40,2048]{2,1,0:T(8,128)(2,1)S(1)} async-done(((bf16[8,40,2048]{2,1,0:T(8,128)(2,1)}), bf16[8,40,2048]{2,1,0:T(8,128)(2,1)S(1)}, u32[]{:S(2)}, u32[]{:S(2)}) %all-to-all-start.1) | async-done | bytes 1310752 | tf_op jit(solution)/shard_map/all_to_all | solution.py:143
  253.1 1.4 gather_fusion
  255.2 4.9 %multiply_reduce_fusion = bf16[128,2048]{1,0:T(8,128)(2,1)} fusion(bf16[128,2,2048]{2,1,0:T(2,128)(2,1)S(1)} %gather.7, pred[128,2]{1,0:T(8,128)(4,1)S(1)} %copy.75, f32[128,2]{1,0:T(8,128)S(1)} %copy.71), kind=kLoop, calls=%fused_computation.28 | loop fusion | flops 1835008 | bytes 1574144 | tf_op jit(solution)/shard_map/reduce_sum | solution.py:153
  (92 shorter events, 10.6 us)
Async XLA Ops:
  7.2 209.7 %copy-start = (bf16[256,2048]{1,0:T(8,128)(2,1)S(1)}, bf16[256,2048]{1,0:T(8,128)(2,1)}, u32[]{:S(2)}) copy-start(bf16[256,2048]{1,0:T(8,128)(2,1)} %param.20) | copy-start | bytes 3145732
  7.2 44.7 %copy-start.3 = (bf16[512,256]{1,0:T(8,128)(2,1)S(1)}, bf16[512,256]{1,0:T(8,128)(2,1)}, u32[]{:S(2)}) copy-start(bf16[512,256]{1,0:T(8,128)(2,1)} %param.17) | copy-start | bytes 786436
  7.2 104.1 %copy-start.4 = (bf16[512,256]{1,0:T(8,128)(2,1)S(1)}, bf16[512,256]{1,0:T(8,128)(2,1)}, u32[]{:S(2)}) copy-start(bf16[512,256]{1,0:T(8,128)(2,1)} %param.16) | copy-start | bytes 786436
  7.2 123.4 %all-gather.5.cloned.1.call-start = ((), (), s32[]{:S(2)}) async-start(), calls=%async_computation.6 | async-start | bytes 6553600 | tf_op jit(solution)/shard_map/all_gather | solution.py:122
  51.8 119.7 %all-gather.3.cloned.1.call-start = ((), (), s32[]{:S(2)}) async-start(), calls=%async_computation.4 | async-start | bytes 2359296 | tf_op jit(solution)/shard_map/all_gather | solution.py:63
  52.0 9.6 %collective-permute-start = (bf16[512,256]{0,1:T(8,128)(2,1)S(1)}, bf16[512,256]{0,1:T(8,128)(2,1)S(1)}, u32[]{:S(2)}, u32[]{:S(2)}) collective-permute-start(bf16[512,256]{0,1:T(8,128)(2,1)S(1)} %copy.64), channel_id=1, source_target_pairs={{0,4},{4,8},{8,12},{12,16},{16,20},{20,24},{24,28},{28,0},{1,5},{5... | collective-permute-start | bytes 786440 | tf_op jit(solution)/shard_map/ppermute | solution.py:67
  61.6 9.1 %collective-permute-start.1 = (bf16[512,256]{0,1:T(8,128)(2,1)S(1)}, bf16[512,256]{0,1:T(8,128)(2,1)S(1)}, u32[]{:S(2)}, u32[]{:S(2)}) collective-permute-start(bf16[512,256]{0,1:T(8,128)(2,1)S(1)} %collective-permute-done), channel_id=1, source_target_pairs={{0,4},{4,8},{8,12},{12,16},{16,20},{20,24},{24,28},{28,0},{1,5},{5... | collective-permute-start | bytes 786440 | tf_op jit(solution)/shard_map/ppermute | solution.py:67
  70.7 9.1 %collective-permute-start.2 = (bf16[512,256]{0,1:T(8,128)(2,1)S(1)}, bf16[512,256]{0,1:T(8,128)(2,1)S(1)}, u32[]{:S(2)}, u32[]{:S(2)}) collective-permute-start(bf16[512,256]{0,1:T(8,128)(2,1)S(1)} %collective-permute-done.1), channel_id=1, source_target_pairs={{0,4},{4,8},{8,12},{12,16},{16,20},{20,24},{24,28},{28,0},{1,5},{5... | collective-permute-start | bytes 786440 | tf_op jit(solution)/shard_map/ppermute | solution.py:67
  79.8 9.4 %collective-permute-start.3 = (bf16[512,256]{0,1:T(8,128)(2,1)S(1)}, bf16[512,256]{0,1:T(8,128)(2,1)S(1)}, u32[]{:S(2)}, u32[]{:S(2)}) collective-permute-start(bf16[512,256]{0,1:T(8,128)(2,1)S(1)} %collective-permute-done.2), channel_id=1, source_target_pairs={{0,4},{4,8},{8,12},{12,16},{16,20},{20,24},{24,28},{28,0},{1,5},{5... | collective-permute-start | bytes 786440 | tf_op jit(solution)/shard_map/ppermute | solution.py:67
  89.2 24.9 %copy-start.1 = (bf16[512,256]{0,1:T(8,128)(2,1)}, bf16[512,256]{0,1:T(8,128)(2,1)S(1)}, u32[]{:S(2)}) copy-start(bf16[512,256]{0,1:T(8,128)(2,1)S(1)} %collective-permute-done.3) | copy-start | bytes 786436
  89.2 10.6 %collective-permute-start.4 = (bf16[512,256]{0,1:T(8,128)(2,1)S(1)}, bf16[512,256]{0,1:T(8,128)(2,1)S(1)}, u32[]{:S(2)}, u32[]{:S(2)}) collective-permute-start(bf16[512,256]{0,1:T(8,128)(2,1)S(1)} %collective-permute-done.3), channel_id=1, source_target_pairs={{0,4},{4,8},{8,12},{12,16},{16,20},{20,24},{24,28},{28,0},{1,5},{5... | collective-permute-start | bytes 786440 | tf_op jit(solution)/shard_map/ppermute | solution.py:67
  99.8 12.4 %copy-start.2 = (bf16[512,256]{0,1:T(8,128)(2,1)}, bf16[512,256]{0,1:T(8,128)(2,1)S(1)}, u32[]{:S(2)}) copy-start(bf16[512,256]{0,1:T(8,128)(2,1)S(1)} %collective-permute-done.4) | copy-start | bytes 786436
  99.8 11.5 %collective-permute-start.5 = (bf16[512,256]{0,1:T(8,128)(2,1)S(1)}, bf16[512,256]{0,1:T(8,128)(2,1)}, u32[]{:S(2)}, u32[]{:S(2)}) collective-permute-start(bf16[512,256]{0,1:T(8,128)(2,1)S(1)} %collective-permute-done.4), channel_id=1, source_target_pairs={{0,4},{4,8},{8,12},{12,16},{16,20},{20,24},{24,28},{28,0},{1,5},{5... | collective-permute-start | bytes 786440 | tf_op jit(solution)/shard_map/ppermute | solution.py:67
  111.3 9.4 %collective-permute-start.6 = (bf16[512,256]{0,1:T(8,128)(2,1)}, bf16[512,256]{0,1:T(8,128)(2,1)}, u32[]{:S(2)}, u32[]{:S(2)}) collective-permute-start(bf16[512,256]{0,1:T(8,128)(2,1)} %collective-permute-done.5), channel_id=1, source_target_pairs={{0,4},{4,8},{8,12},{12,16},{16,20},{20,24},{24,28},{28,0},{1,5},{5... | collective-permute-start | bytes 786440 | tf_op jit(solution)/shard_map/ppermute | solution.py:67
  112.2 107.0 %reduce-scatter.5.cloned.1.call-start = ((), (), s32[]{:S(2)}) async-start(), calls=%async_computation.7 | async-start | bytes 6553600 | tf_op jit(solution)/shard_map/reduce_scatter | solution.py:137
  158.4 101.7 %reduce-scatter.3.cloned.1.call-start = ((), (), s32[]{:S(2)}) async-start(), calls=%async_computation.5 | async-start | bytes 2621440 | tf_op jit(solution)/shard_map/reduce_scatter | solution.py:129
  171.5 45.2 %copy-start.7 = (f32[2]{0:T(128)S(1)}, f32[2]{0:T(128)}, u32[]{:S(2)}) copy-start(f32[2]{0:T(128)} %param.18) | copy-start | bytes 28
  171.5 45.4 %copy-start.8 = (f32[128]{0:T(128)S(1)}, f32[128]{0:T(128)}, u32[]{:S(2)}) copy-start(f32[128]{0:T(128)} %param.19) | copy-start | bytes 1540
  216.9 5.9 %copy-start.5 = (s32[128,2]{0,1:T(2,128)S(1)}, s32[128,2]{0,1:T(2,128)}, u32[]{:S(2)}) copy-start(s32[128,2]{0,1:T(2,128)} %param.23) | copy-start | bytes 3076
  216.9 6.3 %copy-start.6 = (f32[128,2]{0,1:T(2,128)S(1)}, f32[128,2]{0,1:T(2,128)}, u32[]{:S(2)}) copy-start(f32[128,2]{0,1:T(2,128)} %param.24) | copy-start | bytes 3076
  219.2 33.9 %all-to-all-start.1 = ((bf16[8,40,2048]{2,1,0:T(8,128)(2,1)}), bf16[8,40,2048]{2,1,0:T(8,128)(2,1)S(1)}, u32[]{:S(2)}, u32[]{:S(2)}) async-start(bf16[8,40,2048]{2,1,0:T(8,128)(2,1)} %bitcast.103), calls=%async_computation.3 | async-start | bytes 2621440 | tf_op jit(solution)/shard_map/all_to_all | solution.py:143
Sparse Core Ops, SparseCore 0:
  51.9 39.4 all-gather.4
  112.3 51.7 all-gather.2
  166.6 49.5 reduce-scatter.4
  219.3 31.0 reduce-scatter.2
